TPU v7x, 32 devices: a whole 2x2x4 slice. The times are simulated.
32 devices in a mesh: grp: 2 (over y), sp: 4 (over z), tp: 4 (over x, core).
Axes of the slice: x: 2, y: 2, z: 4, core: 2. Of those that a mesh axis runs over, the one named last changes fastest.
Arguments:
- hidden_in: bfloat16 [2048, 2048], P(('grp', 'sp'), 'tp'), parts along dimension 0, may hold values from -40 to 40
- norm_gain: float32 [3, 2048], replicated, may hold values from 0.1 to 1.9
- query_weight: bfloat16 [3, 1024, 2048], P(None, 'tp'), may hold values from -6 to 6
- key_weight: bfloat16 [3, 1024, 2048], P(None, 'tp'), may hold values from -6 to 6
- value_weight: bfloat16 [3, 1024, 2048], P(None, 'tp'), may hold values from -0.125 to 0.125
- output_weight: bfloat16 [3, 1024, 2048], P(None, None, 'tp'), may hold values from -0.75 to 0.75
- offset_bias: float32 [3, 16, 15, 31], P(None, 'tp'), may hold values from -4 to 4
Outputs:
- hidden_out: bfloat16 [2048, 2048], P(('grp', 'sp'), 'tp'), parts along dimension 0
There are 2 independent parts, one for each index of `grp`. A program takes and returns all parts, laid end to end along the dimension named above; an argument that names none is the same for every part. Nothing has to cross between parts.
All inputs are finite; a program needn't handle non-finite values.
Results may differ from a plain program's by a relative error of at most 0.028.
Values may be sent and summed in bfloat16 or wider, within the bound.
A program may use at most 64 MiB of HBM per device.

v0:
```python
import functools

import jax
import jax.numpy as jnp
from jax import lax
from jax.experimental import pallas as pl
from jax.experimental.pallas import tpu as pltpu
from jax.sharding import PartitionSpec as P

HEAD_DIM = 64
GRID_W = 64
ROW_SPAN = 8
COL_SPAN = 16
EPS = 1e-06
NEG = -1e30
CHUNK_ROWS = 2
NT = (((1,), (1,)), ((), ()))


def kernel(
    n_tp, n_sp, hidden, gain, wq, wk, wv, wo, table, out,
    xbuf, att, kv, qbuf, normed, bias, wqkv, wout,
    w_sem, io_sem, xs, xr, xfs, xfr, ats, atr, afs, afr, hs, hr,
):
    layers = wqkv.shape[0]
    tokens, width = hidden.shape
    channels = qbuf.shape[1]
    features = n_tp * width
    rows_dev = tokens // GRID_W
    half = ROW_SPAN // 2
    halo = half * GRID_W
    chunk = CHUNK_ROWS * GRID_W
    chunks = tokens // chunk
    heads = channels // HEAD_DIM
    per_group = 2 if heads % 2 == 0 else 1
    groups = heads // per_group
    lanes = per_group * HEAD_DIM
    span = ROW_SPAN * GRID_W

    sp = lax.axis_index("sp")
    me = lax.axis_index("tp")
    core = lax.rem(me, 2)
    chip = me // 2
    chips = n_tp // 2
    sibling = me + 1 - 2 * core
    all_rows = rows_dev * n_sp
    first_row = sp * rows_dev

    def target(i):
        return lax.rem(chip + i, chips) * 2 + core

    def origin(i):
        return lax.rem(chip - i + chips, chips) * 2 + core

    own_copies = [
        pltpu.make_async_copy(
            hidden.at[pl.ds(c * chunk, chunk)],
            xbuf.at[0, me, pl.ds(c * chunk, chunk)],
            io_sem.at[c],
        )
        for c in range(chunks)
    ]
    for copy in own_copies:
        copy.start()

    def weight_copies(l):
        parts = [
            pltpu.make_async_copy(w.at[l], wqkv.at[l, pl.ds(i * channels, channels)], w_sem.at[l, i])
            for i, w in enumerate((wk, wv, wq))
        ]
        return parts, pltpu.make_async_copy(wo.at[l], wout.at[l], w_sem.at[l, 3])

    for l in range(layers):
        parts, last = weight_copies(l)
        for copy in parts:
            copy.start()
        last.start()

    barrier = pltpu.get_barrier_semaphore()
    for i in range(1, chips):
        pl.semaphore_signal(barrier, inc=1, device_id={"tp": target(i)})
    pl.semaphore_signal(barrier, inc=1, device_id={"tp": sibling})

    @pl.when(sp > 0)
    def _():
        pl.semaphore_signal(barrier, inc=1, device_id={"sp": sp - 1})

    @pl.when(sp < n_sp - 1)
    def _():
        pl.semaphore_signal(barrier, inc=1, device_id={"sp": sp + 1})

    pl.semaphore_wait(barrier, chips + jnp.minimum(sp, 1) + jnp.minimum(n_sp - 1 - sp, 1))

    def remote(buf, l, who, c, send, recv, i, dest):
        part = buf.at[l, who, pl.ds(c * chunk, chunk)]
        return pltpu.make_async_remote_copy(
            src_ref=part,
            dst_ref=part,
            send_sem=send.at[l, c, i],
            recv_sem=recv.at[l, c, i],
            device_id={"tp": dest},
        )

    def spread(buf, l, c, sems):
        for i in range(1, chips):
            remote(buf, l, me, c, sems[0], sems[1], i, target(i)).start()
        remote(buf, l, me, c, sems[0], sems[1], 0, sibling).start()

    def forward(buf, l, c, sems):
        for i in range(1, chips):
            remote(buf, l, origin(i), c, sems[0], sems[1], i, target(i)).wait_recv()
            remote(buf, l, origin(i), c, sems[2], sems[3], i, sibling).start()

    def collect(buf, l, c, sems):
        remote(buf, l, me, c, sems[0], sems[1], 0, sibling).wait_recv()
        for i in range(1, chips):
            remote(buf, l, origin(i), c, sems[2], sems[3], i, sibling).wait_recv()

    def drain(buf, l, c, sems):
        for i in range(chips):
            remote(buf, l, me, c, sems[0], sems[1], i, sibling).wait_send()
        for i in range(1, chips):
            remote(buf, l, me, c, sems[2], sems[3], i, sibling).wait_send()

    x_sems = (xs, xr, xfs, xfr)
    a_sems = (ats, atr, afs, afr)

    def up_copy(l, c):
        low = max(c * chunk, tokens - halo)
        size = (c + 1) * chunk - low
        if size <= 0:
            return None
        return pltpu.make_async_remote_copy(
            src_ref=kv.at[l, :, pl.ds(halo + low, size)],
            dst_ref=kv.at[l, :, pl.ds(low - (tokens - halo), size)],
            send_sem=hs.at[l, c, 0],
            recv_sem=hr.at[l, c, 0],
            device_id={"sp": sp + 1},
        )

    def down_copy(l, c):
        size = min((c + 1) * chunk, halo) - c * chunk
        if size <= 0:
            return None
        return pltpu.make_async_remote_copy(
            src_ref=kv.at[l, :, pl.ds(halo + c * chunk, size)],
            dst_ref=kv.at[l, :, pl.ds(halo + tokens + c * chunk, size)],
            send_sem=hs.at[l, c, 1],
            recv_sem=hr.at[l, c, 1],
            device_id={"sp": sp - 1},
        )

    def when_copy(condition, make, l, c, action):
        copy = make(l, c)
        if copy is None:
            return

        @pl.when(condition)
        def _():
            getattr(copy, action)()

    has_low = sp > 0
    has_high = sp < n_sp - 1

    for c in range(chunks):
        own_copies[c].wait()
        spread(xbuf, 0, c, x_sems)

    q_at = lax.broadcasted_iota(jnp.int32, (GRID_W, 2 * GRID_W), 0)
    k_at = lax.rem(lax.broadcasted_iota(jnp.int32, (GRID_W, 2 * GRID_W), 1), GRID_W)
    w_at = jnp.clip(q_at - COL_SPAN // 2, 0, GRID_W - COL_SPAN)
    inside = (k_at >= w_at) & (k_at < w_at + COL_SPAN)
    lane_low = lax.broadcasted_iota(jnp.int32, (GRID_W, lanes), 1) < HEAD_DIM

    def window_first(r):
        row = first_row + r
        return jnp.clip(row - half, 0, all_rows - ROW_SPAN)

    def make_bias(l):
        for r in range(rows_dev):
            j0 = window_first(r) - (first_row + r) + ROW_SPAN - 1
            for h in range(heads):
                for pair in range(ROW_SPAN // 2):
                    line = table[l, h, pl.ds(j0 + 2 * pair, 1), :]
                    rolled = pltpu.roll(
                        jnp.broadcast_to(line, (GRID_W, 2 * GRID_W)), 0, 1, stride=1, stride_axis=0
                    )
                    bias[
                        r,
                        h // per_group,
                        (h % per_group) * GRID_W : (h % per_group + 1) * GRID_W,
                        pair * 2 * GRID_W : (pair + 1) * 2 * GRID_W,
                    ] = jnp.where(inside, rolled, NEG)

    def project(l, c):
        rows = pl.ds(c * chunk, chunk)
        total = jnp.zeros((chunk, 1), jnp.float32)
        for t in range(n_tp):
            wide = xbuf[l, t, rows, :].astype(jnp.float32)
            total = total + jnp.sum(wide * wide, axis=1, keepdims=True)
        scale = lax.rsqrt(total * (1.0 / features) + EPS)
        for t in range(n_tp):
            cols = slice(t * width, (t + 1) * width)
            wide = xbuf[l, t, rows, :].astype(jnp.float32)
            gain_row = gain[0:1, cols]
            for k in range(1, layers):
                gain_row = jnp.where(l == k, gain[k : k + 1, cols], gain_row)
            normed[:, cols] = (wide * scale * gain_row).astype(jnp.bfloat16)
        made = [
            lax.dot_general(
                normed[...],
                wqkv[l, pl.ds(i * channels, channels), :],
                NT,
                preferred_element_type=jnp.float32,
            )
            for i in range(2)
        ]
        for i in range(2):
            kv[l, i, pl.ds(halo + c * chunk, chunk), :] = made[i].astype(jnp.bfloat16)
        when_copy(has_high, up_copy, l, c, "start")
        when_copy(has_low, down_copy, l, c, "start")
        queries = lax.dot_general(
            normed[...],
            wqkv[l, pl.ds(2 * channels, channels), :],
            NT,
            preferred_element_type=jnp.float32,
        )
        qbuf[rows, :] = (queries.astype(jnp.bfloat16) * HEAD_DIM**-0.5).astype(jnp.bfloat16)

    def attend(l, r):
        start = pl.multiple_of((window_first(r) - first_row + half) * GRID_W, GRID_W)
        rows = pl.ds(r * GRID_W, GRID_W)
        for g in range(groups):
            cols = slice(g * lanes, (g + 1) * lanes)
            query = qbuf[rows, cols]
            if per_group == 2:
                zero = jnp.zeros_like(query)
                query = jnp.concatenate(
                    [jnp.where(lane_low, query, zero), jnp.where(lane_low, zero, query)], axis=0
                )
            score = lax.dot_general(
                query, kv[l, 0, pl.ds(start, span), cols], NT, preferred_element_type=jnp.float32
            )
            score = score + bias[r, g]
            lifted = jnp.exp(score - jnp.max(score, axis=-1, keepdims=True))
            weights = lifted * (1.0 / jnp.sum(lifted, axis=-1, keepdims=True))
            mixed = jnp.dot(
                weights.astype(jnp.bfloat16),
                kv[l, 1, pl.ds(start, span), cols],
                preferred_element_type=jnp.float32,
            )
            if per_group == 2:
                mixed = jnp.where(lane_low, mixed[:GRID_W], mixed[GRID_W:])
            att[l, me, rows, cols] = mixed.astype(jnp.bfloat16)

    def out_copy(c):
        rows = pl.ds(c * chunk, chunk)
        return pltpu.make_async_copy(xbuf.at[layers, me, rows], out.at[rows], io_sem.at[c])

    def layer(l, carry):
        make_bias(l)
        parts, last = weight_copies(l)
        for c in range(chunks):
            forward(xbuf, l, c, x_sems)
            collect(xbuf, l, c, x_sems)
            if c == 0:
                for copy in parts:
                    copy.wait()
            project(l, c)
        for c in range(chunks):
            when_copy(has_low, up_copy, l, c, "wait_recv")
            when_copy(has_high, down_copy, l, c, "wait_recv")
        for r in range(rows_dev):
            attend(l, r)
            if (r + 1) % CHUNK_ROWS == 0:
                spread(att, l, r // CHUNK_ROWS, a_sems)
        last.wait()
        for c in range(chunks):
            rows = pl.ds(c * chunk, chunk)
            forward(att, l, c, a_sems)
            collect(att, l, c, a_sems)
            total = xbuf[l, me, rows, :].astype(jnp.float32)
            for t in range(n_tp):
                total = total + jnp.dot(
                    att[l, t, rows, :],
                    wout[l, t * channels : (t + 1) * channels, :],
                    preferred_element_type=jnp.float32,
                )
            xbuf[l + 1, me, rows, :] = total.astype(jnp.bfloat16)

            @pl.when(l + 1 < layers)
            def _():
                spread(xbuf, l + 1, c, x_sems)

            @pl.when(l + 1 == layers)
            def _():
                out_copy(c).start()

        return carry

    lax.fori_loop(0, layers, layer, 0)

    def finish(l, carry):
        for c in range(chunks):
            drain(xbuf, l, c, x_sems)
            drain(att, l, c, a_sems)
            when_copy(has_high, up_copy, l, c, "wait_send")
            when_copy(has_low, down_copy, l, c, "wait_send")
        return carry

    lax.fori_loop(0, layers, finish, 0)
    for c in range(chunks):
        out_copy(c).wait()


def bias_lines(offset_bias):
    spread = COL_SPAN - 1
    after = jnp.pad(offset_bias[:, :, 1:], ((0, 0), (0, 0), (0, 1), (0, 0)))
    gap = jnp.zeros(offset_bias.shape[:3] + (GRID_W - 2 * spread - 1,), jnp.float32)
    return jnp.concatenate(
        [offset_bias[..., spread:], gap, after, gap, offset_bias[..., :spread]], axis=-1
    )


def solution(mesh):
    n_tp, n_sp = mesh.shape["tp"], mesh.shape["sp"]

    def body(hidden, gain, wq, wk, wv, wo, offset_bias):
        tokens, width = hidden.shape
        layers, channels, features = wq.shape
        heads = channels // HEAD_DIM
        per_group = 2 if heads % 2 == 0 else 1
        rows_dev = tokens // GRID_W
        chunks = rows_dev // CHUNK_ROWS
        chips = n_tp // 2
        halo = ROW_SPAN // 2 * GRID_W
        any_spec = pl.BlockSpec(memory_space=pl.ANY)
        vmem_spec = pl.BlockSpec(memory_space=pltpu.VMEM)
        bf16 = jnp.bfloat16
        hop = pltpu.SemaphoreType.DMA((layers, chunks, chips))
        return pl.pallas_call(
            functools.partial(kernel, n_tp, n_sp),
            out_shape=jax.ShapeDtypeStruct((tokens, width), bf16),
            in_specs=[any_spec, vmem_spec] + [any_spec] * 4 + [vmem_spec],
            out_specs=any_spec,
            scratch_shapes=[
                pltpu.VMEM((layers + 1, n_tp, tokens, width), bf16),
                pltpu.VMEM((layers, n_tp, tokens, channels), bf16),
                pltpu.VMEM((layers, 2, tokens + 2 * halo, channels), bf16),
                pltpu.VMEM((tokens, channels), bf16),
                pltpu.VMEM((CHUNK_ROWS * GRID_W, features), bf16),
                pltpu.VMEM(
                    (rows_dev, heads // per_group, per_group * GRID_W, ROW_SPAN * GRID_W),
                    jnp.float32,
                ),
                pltpu.VMEM((layers, 3 * channels, features), bf16),
                pltpu.VMEM((layers, n_tp * channels, width), bf16),
                pltpu.SemaphoreType.DMA((layers, 4)),
                pltpu.SemaphoreType.DMA((chunks,)),
            ]
            + [hop] * 8
            + [pltpu.SemaphoreType.DMA((layers, chunks, 2))] * 2,
            compiler_params=pltpu.CompilerParams(
                collective_id=0, has_side_effects=True, vmem_limit_bytes=60 * 2**20
            ),
        )(hidden, gain, wq, wk, wv, wo, bias_lines(offset_bias))

    return jax.shard_map(
        body,
        mesh=mesh,
        in_specs=(
            P(("grp", "sp"), "tp"),
            P(),
            P(None, "tp", None),
            P(None, "tp", None),
            P(None, "tp", None),
            P(None, None, "tp"),
            P(None, "tp", None, None),
        ),
        out_specs=P(("grp", "sp"), "tp"),
        check_vma=False,
    )
```

profile of v0, /device:TPU:0, one launch (start us, length us, event | category | flops | bytes accessed | tf_op | source)
XLA Modules:
  0.0 78.8 jit_solution(15367393126856967777)
XLA Ops:
  0.0 0.9 %slice.10 = f32[3,4,14,31]{3,1,2,0:T(4,128)S(1)} slice(f32[3,4,15,31]{3,1,2,0:T(4,128)} %param.13), slice={[0:3], [0:4], [1:15], [0:31]} | slice | bytes 41664 | tf_op jit(solution)/shard_map/slice | solution.py:318
  0.9 1.0 %slice.9 = f32[3,4,15,16]{3,1,2,0:T(4,128)S(1)} slice(f32[3,4,15,31]{3,1,2,0:T(4,128)} %param.13), slice={[0:3], [0:4], [0:15], [15:31]} | slice | bytes 23040 | tf_op jit(solution)/shard_map/slice | solution.py:321
  2.0 0.9 %copy.13 = f32[3,4,15,15]{3,2,1,0:T(8,128)S(1)} copy(f32[3,4,15,15]{3,1,2,0:T(4,128)} %bitcast.1) | data formatting | bytes 21600
  2.9 0.8 %concatenate.3.table = f32[3,4,15,128]{3,2,1,0:T(8,128)} concatenate(f32[3,4,15,16]{3,2,1,0:T(8,128)S(1)} %copy.11, f32[3,4,15,33]{3,2,1,0:T(8,128)S(1)} %broadcast_in_dim.3, f32[3,4,15,31]{3,2,1,0:T(8,128)S(1)} %pad.4, f32[3,4,15,33]{3,2,1,0:T(8,128)S(1)} %broadcast_in_dim.3, f32[3,4,15,15]{3,2,1,0:T(8,128)S(1)} %copy.13), dimensions={3} | concatenate | bytes 184320 | tf_op jit(solution)/shard_map/concatenate | solution.py:320
  3.7 73.5 %shard_map.73 = bf16[256,512]{1,0:T(8,128)(2,1)} custom-call(bf16[256,512]{1,0:T(8,128)(2,1)} %hidden.1, f32[3,2048]{1,0:T(4,128)} %gain.1, bf16[3,256,2048]{2,1,0:T(8,128)(2,1)} %wq.1, bf16[3,256,2048]{2,1,0:T(8,128)(2,1)} %wk.1, bf16[3,256,2048]{2,1,0:T(8,128)(2,1)} %wv.1, bf16[3,1024,512]{2,1,0:T(8,128)(2,1)} %wo.1, f32[3,4,15,128]{3,2,1,0:T(8,128)} %concatenate.3.table), custom_call_target="tpu_custom_call" | custom-call | tf_op jit(solution)/shard_map/pallas_call | solution.py:341
  77.2 1.7 %copy.15 = bf16[256,512]{1,0:T(8,128)(2,1)} copy(bf16[256,512]{1,0:T(8,128)(2,1)} %shard_map.73) | data formatting | bytes 524288
  (4 shorter events, 0.0 us)
where the time goes:
time: 79.1 us; the launch traced here: 78.8 us
  Pallas kernels  73.5 us (93%)
  local copies, waits for them, and re-layouts  5.32 us (7%)
    pallas_call x1, Pallas kernels, body(): pl.pallas_call(functools.partial(kernel, n_tp, n_sp), out_shape=jax.Shape...  73.5 us
    unnamed x4, local copies, waits for them, and re-layouts  2.6 us

commit v1 on v0

--- a/solution.py
+++ b/solution.py
@@ -13,13 +13,13 @@
 COL_SPAN = 16
 EPS = 1e-06
 NEG = -1e30
-CHUNK_ROWS = 2
+CHUNK_ROWS = 1
 NT = (((1,), (1,)), ((), ()))
 
 
 def kernel(
     n_tp, n_sp, hidden, gain, wq, wk, wv, wo, table, out,
-    xbuf, att, kv, qbuf, normed, bias, wqkv, wout,
+    xbuf, att, kv, qbuf, scaled, squares, kv_sum, q_sum, out_sum, lines, bias, wqkv, wout,
     w_sem, io_sem, xs, xr, xfs, xfr, ats, atr, afs, afr, hs, hr,
 ):
     layers = wqkv.shape[0]
@@ -49,8 +49,11 @@
     def target(i):
         return lax.rem(chip + i, chips) * 2 + core
 
+    def origin_chip(i):
+        return lax.rem(chip - i + chips, chips)
+
     def origin(i):
-        return lax.rem(chip - i + chips, chips) * 2 + core
+        return origin_chip(i) * 2 + core
 
     own_copies = [
         pltpu.make_async_copy(
@@ -111,8 +114,11 @@
             remote(buf, l, origin(i), c, sems[0], sems[1], i, target(i)).wait_recv()
             remote(buf, l, origin(i), c, sems[2], sems[3], i, sibling).start()
 
+    def collect_own(buf, l, sems):
+        for c in range(chunks):
+            remote(buf, l, me, c, sems[0], sems[1], 0, sibling).wait_recv()
+
     def collect(buf, l, c, sems):
-        remote(buf, l, me, c, sems[0], sems[1], 0, sibling).wait_recv()
         for i in range(1, chips):
             remote(buf, l, origin(i), c, sems[2], sems[3], i, sibling).wait_recv()
 
@@ -177,11 +183,18 @@
         return jnp.clip(row - half, 0, all_rows - ROW_SPAN)
 
     def make_bias(l):
+        lines[...] = jnp.zeros_like(lines)
+        for j in range(2 * ROW_SPAN - 1):
+            lines[j, :, : 2 * COL_SPAN - 1] = table[l, j]
+        for j in range(2 * ROW_SPAN - 2):
+            lines[j] = pltpu.roll(lines[j], 2 * GRID_W - COL_SPAN + 1, 1) + pltpu.roll(
+                lines[j + 1], GRID_W - COL_SPAN + 1, 1
+            )
         for r in range(rows_dev):
             j0 = window_first(r) - (first_row + r) + ROW_SPAN - 1
             for h in range(heads):
                 for pair in range(ROW_SPAN // 2):
-                    line = table[l, h, pl.ds(j0 + 2 * pair, 1), :]
+                    line = lines[j0 + 2 * pair, h : h + 1, :]
                     rolled = pltpu.roll(
                         jnp.broadcast_to(line, (GRID_W, 2 * GRID_W)), 0, 1, stride=1, stride_axis=0
                     )
@@ -192,40 +205,59 @@
                         pair * 2 * GRID_W : (pair + 1) * 2 * GRID_W,
                     ] = jnp.where(inside, rolled, NEG)
 
-    def project(l, c):
-        rows = pl.ds(c * chunk, chunk)
-        total = jnp.zeros((chunk, 1), jnp.float32)
-        for t in range(n_tp):
-            wide = xbuf[l, t, rows, :].astype(jnp.float32)
-            total = total + jnp.sum(wide * wide, axis=1, keepdims=True)
-        scale = lax.rsqrt(total * (1.0 / features) + EPS)
-        for t in range(n_tp):
-            cols = slice(t * width, (t + 1) * width)
-            wide = xbuf[l, t, rows, :].astype(jnp.float32)
+    def columns(i):
+        return pl.ds(pl.multiple_of(origin_chip(i) * 2 * width, 2 * width), 2 * width)
+
+    def prepare(l, i, rows):
+        total = squares[rows, :] if i else jnp.zeros((tokens, 1), jnp.float32)
+        for u in range(2):
+            at = origin_chip(i) * 2 + u
+            cols = pl.ds(pl.multiple_of(at * width, width), width)
             gain_row = gain[0:1, cols]
             for k in range(1, layers):
                 gain_row = jnp.where(l == k, gain[k : k + 1, cols], gain_row)
-            normed[:, cols] = (wide * scale * gain_row).astype(jnp.bfloat16)
-        made = [
-            lax.dot_general(
-                normed[...],
-                wqkv[l, pl.ds(i * channels, channels), :],
-                NT,
-                preferred_element_type=jnp.float32,
-            )
-            for i in range(2)
-        ]
-        for i in range(2):
-            kv[l, i, pl.ds(halo + c * chunk, chunk), :] = made[i].astype(jnp.bfloat16)
+            wide = xbuf[l, at, rows, :].astype(jnp.float32)
+            total = total + jnp.sum(wide * wide, axis=1, keepdims=True)
+            slot = (2 * i + u) * width
+            scaled[rows, slot : slot + width] = (wide * gain_row).astype(jnp.bfloat16)
+        squares[rows, :] = total
+
+    def product(l, i, rows, first, count):
+        return lax.dot_general(
+            scaled[rows, 2 * i * width : 2 * (i + 1) * width],
+            wqkv[l, pl.ds(first, count), columns(i)],
+            NT,
+            preferred_element_type=jnp.float32,
+        )
+
+    def project_own(l):
+        rows = pl.ds(0, tokens)
+        prepare(l, 0, rows)
+        kv_sum[...] = product(l, 0, rows, 0, 2 * channels)
+        q_sum[...] = product(l, 0, rows, 2 * channels, channels)
+
+    def scale_of(rows):
+        return lax.rsqrt(squares[rows, :] * (1.0 / features) + EPS)
+
+    def project_kv(l, c):
+        rows = pl.ds(c * chunk, chunk)
+        total = kv_sum[rows, :]
+        for i in range(1, chips):
+            prepare(l, i, rows)
+            total = total + product(l, i, rows, 0, 2 * channels)
+        made = (total * scale_of(rows)).astype(jnp.bfloat16)
+        for k in range(2):
+            kv[l, k, pl.ds(halo + c * chunk, chunk), :] = made[:, k * channels : (k + 1) * channels]
         when_copy(has_high, up_copy, l, c, "start")
         when_copy(has_low, down_copy, l, c, "start")
-        queries = lax.dot_general(
-            normed[...],
-            wqkv[l, pl.ds(2 * channels, channels), :],
-            NT,
-            preferred_element_type=jnp.float32,
-        )
-        qbuf[rows, :] = (queries.astype(jnp.bfloat16) * HEAD_DIM**-0.5).astype(jnp.bfloat16)
+
+    def project_q(l):
+        rows = pl.ds(0, tokens)
+        total = q_sum[...]
+        for i in range(1, chips):
+            total = total + product(l, i, rows, 2 * channels, channels)
+        queries = (total * scale_of(rows)).astype(jnp.bfloat16)
+        qbuf[...] = (queries * HEAD_DIM**-0.5).astype(jnp.bfloat16)
 
     def attend(l, r):
         start = pl.multiple_of((window_first(r) - first_row + half) * GRID_W, GRID_W)
@@ -243,9 +275,9 @@
             )
             score = score + bias[r, g]
             lifted = jnp.exp(score - jnp.max(score, axis=-1, keepdims=True))
-            weights = lifted * (1.0 / jnp.sum(lifted, axis=-1, keepdims=True))
-            mixed = jnp.dot(
-                weights.astype(jnp.bfloat16),
+            share = 1.0 / jnp.sum(lifted, axis=-1, keepdims=True)
+            mixed = share * jnp.dot(
+                lifted.astype(jnp.bfloat16),
                 kv[l, 1, pl.ds(start, span), cols],
                 preferred_element_type=jnp.float32,
             )
@@ -257,16 +289,52 @@
         rows = pl.ds(c * chunk, chunk)
         return pltpu.make_async_copy(xbuf.at[layers, me, rows], out.at[rows], io_sem.at[c])
 
+    def project_out_own(l):
+        total = xbuf[l, me].astype(jnp.float32)
+        for u in range(2):
+            total = total + out_part(l, chip * 2 + u, pl.ds(0, tokens))
+        out_sum[...] = total
+
+    def out_part(l, at, rows):
+        return jnp.dot(
+            att[l, at, rows, :],
+            wout[l, pl.ds(pl.multiple_of(at * channels, channels), channels), :],
+            preferred_element_type=jnp.float32,
+        )
+
+    def project_out(l, c):
+        rows = pl.ds(c * chunk, chunk)
+        total = out_sum[rows, :]
+        for i in range(1, chips):
+            for u in range(2):
+                total = total + out_part(l, origin_chip(i) * 2 + u, rows)
+        xbuf[l + 1, me, rows, :] = total.astype(jnp.bfloat16)
+
+        @pl.when(l + 1 < layers)
+        def _():
+            spread(xbuf, l + 1, c, x_sems)
+
+        @pl.when(l + 1 == layers)
+        def _():
+            out_copy(c).start()
+
+    def arrive(buf, l, sems, use):
+        for c in range(chunks + 1):
+            if c < chunks:
+                forward(buf, l, c, sems)
+            if c > 0:
+                collect(buf, l, c - 1, sems)
+                use(l, c - 1)
+
     def layer(l, carry):
         make_bias(l)
         parts, last = weight_copies(l)
-        for c in range(chunks):
-            forward(xbuf, l, c, x_sems)
-            collect(xbuf, l, c, x_sems)
-            if c == 0:
-                for copy in parts:
-                    copy.wait()
-            project(l, c)
+        for copy in parts:
+            copy.wait()
+        collect_own(xbuf, l, x_sems)
+        project_own(l)
+        arrive(xbuf, l, x_sems, project_kv)
+        project_q(l)
         for c in range(chunks):
             when_copy(has_low, up_copy, l, c, "wait_recv")
             when_copy(has_high, down_copy, l, c, "wait_recv")
@@ -275,27 +343,9 @@
             if (r + 1) % CHUNK_ROWS == 0:
                 spread(att, l, r // CHUNK_ROWS, a_sems)
         last.wait()
-        for c in range(chunks):
-            rows = pl.ds(c * chunk, chunk)
-            forward(att, l, c, a_sems)
-            collect(att, l, c, a_sems)
-            total = xbuf[l, me, rows, :].astype(jnp.float32)
-            for t in range(n_tp):
-                total = total + jnp.dot(
-                    att[l, t, rows, :],
-                    wout[l, t * channels : (t + 1) * channels, :],
-                    preferred_element_type=jnp.float32,
-                )
-            xbuf[l + 1, me, rows, :] = total.astype(jnp.bfloat16)
-
-            @pl.when(l + 1 < layers)
-            def _():
-                spread(xbuf, l + 1, c, x_sems)
-
-            @pl.when(l + 1 == layers)
-            def _():
-                out_copy(c).start()
-
+        collect_own(att, l, a_sems)
+        project_out_own(l)
+        arrive(att, l, a_sems, project_out)
         return carry
 
     lax.fori_loop(0, layers, layer, 0)
@@ -311,15 +361,6 @@
     lax.fori_loop(0, layers, finish, 0)
     for c in range(chunks):
         out_copy(c).wait()
-
-
-def bias_lines(offset_bias):
-    spread = COL_SPAN - 1
-    after = jnp.pad(offset_bias[:, :, 1:], ((0, 0), (0, 0), (0, 1), (0, 0)))
-    gap = jnp.zeros(offset_bias.shape[:3] + (GRID_W - 2 * spread - 1,), jnp.float32)
-    return jnp.concatenate(
-        [offset_bias[..., spread:], gap, after, gap, offset_bias[..., :spread]], axis=-1
-    )
 
 
 def solution(mesh):
@@ -348,7 +389,12 @@
                 pltpu.VMEM((layers, n_tp, tokens, channels), bf16),
                 pltpu.VMEM((layers, 2, tokens + 2 * halo, channels), bf16),
                 pltpu.VMEM((tokens, channels), bf16),
-                pltpu.VMEM((CHUNK_ROWS * GRID_W, features), bf16),
+                pltpu.VMEM((tokens, features), bf16),
+                pltpu.VMEM((tokens, 1), jnp.float32),
+                pltpu.VMEM((tokens, 2 * channels), jnp.float32),
+                pltpu.VMEM((tokens, channels), jnp.float32),
+                pltpu.VMEM((tokens, width), jnp.float32),
+                pltpu.VMEM((2 * ROW_SPAN - 1, heads, 2 * GRID_W), jnp.float32),
                 pltpu.VMEM(
                     (rows_dev, heads // per_group, per_group * GRID_W, ROW_SPAN * GRID_W),
                     jnp.float32,
@@ -363,7 +409,7 @@
             compiler_params=pltpu.CompilerParams(
                 collective_id=0, has_side_effects=True, vmem_limit_bytes=60 * 2**20
             ),
-        )(hidden, gain, wq, wk, wv, wo, bias_lines(offset_bias))
+        )(hidden, gain, wq, wk, wv, wo, jnp.transpose(offset_bias, (0, 2, 1, 3)))
 
     return jax.shard_map(
         body,

time: 79.1 us -> 69.8 us (0.88)
  Pallas kernels: 73.5 us -> 67.9 us
  local copies, waits for them, and re-layouts: 5.32 us -> 1.67 us
    pallas_call x1, Pallas kernels: 73.5 us -> 67.9 us  [body(): pl.pallas_call(functools.partial(kernel, n_tp, n_sp), out_shape=jax.Shape...]
    slice x2 -> x0, local copies, waits for them, and re-layouts: 1.89 us -> none  [the longest x1 1 us: bias_lines(): offset_bias[..., spread:]]
    unnamed x4 -> x1, local copies, waits for them, and re-layouts: 2.6 us -> 1.67 us
    concatenate x1 -> x0, local copies, waits for them, and re-layouts: 0.81 us -> none  [bias_lines(): jnp.concatenate([offset_bias[..., spread:], gap, after, gap, offset_bias[...]
where the time goes in v1:
time: 69.8 us; the launch traced here: 69.6 us
  Pallas kernels  67.9 us (97%)
  local copies, waits for them, and re-layouts  1.67 us (2%)
    pallas_call x1, Pallas kernels, body(): pl.pallas_call(functools.partial(kernel, n_tp, n_sp), out_shape=jax.Shape...  67.9 us
    unnamed x1, local copies, waits for them, and re-layouts  1.67 us

profile of v1, /device:TPU:0, one launch (start us, length us, event | category | flops | bytes accessed | tf_op | source)
XLA Modules:
  0.0 69.6 jit_solution(17535880330683198859)
XLA Ops:
  0.0 67.9 %shard_map.73 = bf16[256,512]{1,0:T(8,128)(2,1)} custom-call(bf16[256,512]{1,0:T(8,128)(2,1)} %hidden.1, f32[3,2048]{1,0:T(4,128)} %gain.1, bf16[3,256,2048]{2,1,0:T(8,128)(2,1)} %wq.1, bf16[3,256,2048]{2,1,0:T(8,128)(2,1)} %wk.1, bf16[3,256,2048]{2,1,0:T(8,128)(2,1)} %wv.1, bf16[3,1024,512]{2,1,0:T(8,128)(2,1)} %wo.1, f32[3,15,4,31]{3,2,1,0:T(4,128)} %bitcast.1), custom_call_target="tpu_custom_call" | custom-call | tf_op jit(solution)/shard_map/pallas_call | solution.py:382
  68.0 1.7 %copy.9 = bf16[256,512]{1,0:T(8,128)(2,1)} copy(bf16[256,512]{1,0:T(8,128)(2,1)} %shard_map.73) | data formatting | bytes 524288

commit v2 on v1

--- a/solution.py
+++ b/solution.py
@@ -73,11 +73,13 @@
         ]
         return parts, pltpu.make_async_copy(wo.at[l], wout.at[l], w_sem.at[l, 3])
 
-    for l in range(layers):
+    def fetch_weights(l):
         parts, last = weight_copies(l)
         for copy in parts:
             copy.start()
         last.start()
+
+    fetch_weights(0)
 
     barrier = pltpu.get_barrier_semaphore()
     for i in range(1, chips):
@@ -167,6 +169,9 @@
 
     has_low = sp > 0
     has_high = sp < n_sp - 1
+
+    def down_used(sender, c):
+        return sender == 1 if c * chunk >= halo - GRID_W else sender > 0
 
     for c in range(chunks):
         own_copies[c].wait()
@@ -249,7 +254,7 @@
         for k in range(2):
             kv[l, k, pl.ds(halo + c * chunk, chunk), :] = made[:, k * channels : (k + 1) * channels]
         when_copy(has_high, up_copy, l, c, "start")
-        when_copy(has_low, down_copy, l, c, "start")
+        when_copy(down_used(sp, c), down_copy, l, c, "start")
 
     def project_q(l):
         rows = pl.ds(0, tokens)
@@ -331,13 +336,18 @@
         parts, last = weight_copies(l)
         for copy in parts:
             copy.wait()
+
+        @pl.when(l + 1 < layers)
+        def _():
+            fetch_weights(l + 1)
+
         collect_own(xbuf, l, x_sems)
         project_own(l)
         arrive(xbuf, l, x_sems, project_kv)
         project_q(l)
         for c in range(chunks):
             when_copy(has_low, up_copy, l, c, "wait_recv")
-            when_copy(has_high, down_copy, l, c, "wait_recv")
+            when_copy(down_used(sp + 1, c) & has_high, down_copy, l, c, "wait_recv")
         for r in range(rows_dev):
             attend(l, r)
             if (r + 1) % CHUNK_ROWS == 0:
@@ -355,7 +365,7 @@
             drain(xbuf, l, c, x_sems)
             drain(att, l, c, a_sems)
             when_copy(has_high, up_copy, l, c, "wait_send")
-            when_copy(has_low, down_copy, l, c, "wait_send")
+            when_copy(down_used(sp, c), down_copy, l, c, "wait_send")
         return carry
 
     lax.fori_loop(0, layers, finish, 0)

time: 69.8 us -> 66.5 us (0.953)
  Pallas kernels: 67.9 us -> 64.7 us
    pallas_call x1, Pallas kernels: 67.9 us -> 64.7 us  [body(): pl.pallas_call(functools.partial(kernel, n_tp, n_sp), out_shape=jax.Shape...]
where the time goes in v2:
time: 66.5 us; the launch traced here: 66.4 us
  Pallas kernels  64.7 us (97%)
  local copies, waits for them, and re-layouts  1.67 us (3%)
    pallas_call x1, Pallas kernels, body(): pl.pallas_call(functools.partial(kernel, n_tp, n_sp), out_shape=jax.Shape...  64.7 us
    unnamed x1, local copies, waits for them, and re-layouts  1.67 us

profile of v2, /device:TPU:0, one launch (start us, length us, event | category | flops | bytes accessed | tf_op | source)
XLA Modules:
  0.0 66.4 jit_solution(12637069290538409009)
XLA Ops:
  0.0 64.7 %shard_map.73 = bf16[256,512]{1,0:T(8,128)(2,1)} custom-call(bf16[256,512]{1,0:T(8,128)(2,1)} %hidden.1, f32[3,2048]{1,0:T(4,128)} %gain.1, bf16[3,256,2048]{2,1,0:T(8,128)(2,1)} %wq.1, bf16[3,256,2048]{2,1,0:T(8,128)(2,1)} %wk.1, bf16[3,256,2048]{2,1,0:T(8,128)(2,1)} %wv.1, bf16[3,1024,512]{2,1,0:T(8,128)(2,1)} %wo.1, f32[3,15,4,31]{3,2,1,0:T(4,128)} %bitcast.1), custom_call_target="tpu_custom_call" | custom-call | tf_op jit(solution)/shard_map/pallas_call | solution.py:392
  64.7 1.7 %copy.9 = bf16[256,512]{1,0:T(8,128)(2,1)} copy(bf16[256,512]{1,0:T(8,128)(2,1)} %shard_map.73) | data formatting | bytes 524288
